TPU v7x, 128 devices: a whole 4x4x4 slice. The times are simulated.
128 devices in a mesh: sp: 16 (over z, y), dp: 8 (over x, core).
Axes of the slice: x: 4, y: 4, z: 4, core: 2. Of those that a mesh axis runs over, the one named last changes fastest.
Arguments:
- u_pre: bfloat16 [8, 16384, 2048], P('dp', 'sp'), may hold values from -6 to 6
- v_pre: bfloat16 [8, 16384, 2048], P('dp', 'sp'), may hold values from -6 to 6
- d_out: bfloat16 [8, 16384, 2048], P('dp', 'sp'), may hold values from -6 to 6
- w_mix: bfloat16 [16, 128, 128], replicated, may hold values from -0.5 to 0.5
- mix_bias: float32 [16, 128], replicated, may hold values from 0.1 to 1.9
- norm_gain: float32 [16, 128], replicated, may hold values from 0.1 to 1.9
- norm_shift: float32 [16, 128], replicated, may hold values from -3 to 3
- w_out: bfloat16 [2048, 2048], P('dp'), may hold values from -0.125 to 0.125
Outputs:
- grad_u: bfloat16 [8, 16384, 2048], P('dp', 'sp')
- grad_v: bfloat16 [8, 16384, 2048], P('dp', 'sp')
- grad_w_out: float32 [2048, 2048], P('dp')
- grad_w_mix: float32 [16, 128, 128], replicated
- grad_mix_bias: float32 [16, 128], replicated
- grad_gain: float32 [16, 128], replicated
- grad_shift: float32 [16, 128], replicated
All inputs are finite; a program needn't handle non-finite values.
Results may differ from a plain program's by a relative error of at most 0.012.
Values may be sent and summed in bfloat16 or wider, within the bound.
No kernel may reach another device: no remote copies, remote signals or barrier semaphores. Data moves between devices by JAX's collectives and lax.ppermute only.
A program may use at most 192 MiB of HBM per device.

v0:
```python
import functools

import jax
import jax.numpy as jnp
from jax import lax
from jax.experimental import pallas as pl
from jax.experimental.pallas import tpu as pltpu
from jax.sharding import Mesh, PartitionSpec as P

EPS = 1e-05
C0 = 0.7978845608028654
C1 = C0 * 0.044715
F32 = jnp.float32
BF16 = jnp.bfloat16
BLK = 128
PAIR = 256
SIDE = 16
PACK = 9 * BLK
ROOT = BLK**0.5


def tanh_of(a):
    a2 = a * a
    return jnp.tanh(a * (C0 + C1 * a2)), a2


def gelu(a):
    t, _ = tanh_of(a)
    return a * (0.5 + 0.5 * t)


def gelu_and_slope(a):
    t, a2 = tanh_of(a)
    half = 0.5 + 0.5 * t
    value = a * half
    return value, half + value * (1.0 - half) * (2.0 * C0 + (6.0 * C1) * a2)


def norm(gated):
    centre = gated - jnp.mean(gated, axis=-1, keepdims=True)
    inverse = lax.rsqrt(jnp.sum(centre * centre, axis=-1, keepdims=True) + BLK * EPS)
    return centre * inverse, inverse


def lower_of(a):
    row = lax.broadcasted_iota(jnp.int32, a.shape, 0)
    col = lax.broadcasted_iota(jnp.int32, a.shape, 1)
    return jnp.where(row >= col, a, jnp.zeros_like(a))


def upright(row):
    return jnp.broadcast_to(row, (BLK, BLK)).T


def columns(ref, at, first=0, count=None):
    count = ref.shape[0] if count is None else count
    return jnp.concatenate([ref[first + k, at] for k in range(count)], axis=1)


def scatter_columns(src, dst, sem):
    @pl.loop(0, dst.shape[0])
    def _(k):
        at = pl.ds(pl.multiple_of(k * BLK, BLK), BLK)
        pltpu.make_async_copy(src.at[:, at], dst.at[k], sem).start()


def await_all(dst, sem):
    pltpu.make_async_copy(dst, dst, sem).wait()


def cols_of(g):
    return slice(g * BLK, (g + 1) * BLK)


def forward_kernel(
    order, u_ref, v_ref, d_hbm, w_ref, bias_ref, gain_ref, shift_ref, out_ref, d_ref, go_ref, low_at, bias_at, sem
):
    blocks, length, _ = d_ref.shape
    turns = length // PAIR
    step = pl.program_id(0)
    last = pl.num_programs(0) - 1
    now, before = lax.rem(step, 2), lax.rem(step + 1, 2)
    part = blocks // turns

    def multiply(i):
        out_ref[0, :, i * part * BLK : (i + 1) * part * BLK] = jnp.dot(
            go_ref[before],
            columns(d_ref, slice(None), i * part, part),
            preferred_element_type=F32,
        ).astype(out_ref.dtype)

    def gate(i):
        rows = [slice(i * PAIR + h * BLK, i * PAIR + (h + 1) * BLK) for h in range(2)]
        for g in range(2):
            gain, shift = ROOT * gain_ref[0, g : g + 1], shift_ref[0, g : g + 1]
            normed = []
            for at in rows:
                scaled, _ = norm(gelu(v_ref[at, cols_of(g)].astype(F32)))
                normed.append((scaled * gain + shift).astype(BF16))
            mixed = jnp.dot(
                low_at[g], jnp.concatenate(normed, axis=1), preferred_element_type=F32
            )
            for h, at in enumerate(rows):
                upper = gelu(u_ref[at, cols_of(g)].astype(F32))
                gated_out = (upper * (mixed[:, cols_of(h)] + bias_at[g])).astype(BF16)
                go_ref[now, cols_of(g), at] = gated_out.T

    @pl.when(step == 0)
    def _():
        scatter_columns(d_hbm, d_ref, sem)

    for g in range(2):
        bias_at[g] = upright(bias_ref[0, g : g + 1])
        low_at[g] = lower_of(w_ref[0, g].astype(F32)).astype(BF16)

    @pl.when(step == 0)
    def _():
        for i in range(turns):
            gate(i)
        await_all(d_ref, sem)

    @pl.when((step > 0) & (step < last))
    def _():
        for i in range(turns):
            multiply(i)
            gate(i)

    @pl.when(step == last)
    def _():
        for i in range(turns):
            multiply(i)


def forward(here, theirs, u, v, d, mix, bias, gain, shift):
    length, width = u.shape
    n = width // PAIR // 2
    last = n - 1
    pair_at = lambda j, o: 2 * jnp.minimum(j, last) + (1 - o[1] if theirs else o[1])
    cur = lambda j, o: (0, pair_at(j, o))
    par = lambda j, o: (pair_at(j, o), 0, 0)
    return pl.pallas_call(
        forward_kernel,
        grid_spec=pltpu.PrefetchScalarGridSpec(
            num_scalar_prefetch=1,
            grid=(n + 1,),
            in_specs=[
                pl.BlockSpec((length, PAIR), cur),
                pl.BlockSpec((length, PAIR), cur),
                pl.BlockSpec(memory_space=pl.ANY),
                pl.BlockSpec((1, 2, BLK, BLK), lambda j, o: (pair_at(j, o), 0, 0, 0)),
                pl.BlockSpec((1, 2, BLK), par),
                pl.BlockSpec((1, 2, BLK), par),
                pl.BlockSpec((1, 2, BLK), par),
            ],
            out_specs=pl.BlockSpec((1, PAIR, width), lambda j, o: (jnp.maximum(j - 1, 0), 0, 0)),
            scratch_shapes=[
                pltpu.VMEM((width // BLK, length, BLK), BF16),
                pltpu.VMEM((2, PAIR, length), BF16),
                pltpu.VMEM((2, BLK, BLK), BF16),
                pltpu.VMEM((2, BLK, BLK), F32),
                pltpu.SemaphoreType.DMA,
            ],
        ),
        out_shape=jax.ShapeDtypeStruct((n, PAIR, width), BF16),
        cost_estimate=pl.CostEstimate(
            flops=2 * n * PAIR * length * (width + BLK) * 2,
            bytes_accessed=length * width * 2 + n * PAIR * (4 * length + 2 * width),
            transcendentals=2 * n * PAIR * length,
        ),
        name="fwd",
    )(here, u, v, d, mix, bias, gain, shift)


def backward_kernel(
    pieces, order, u_ref, v_ref, d_hbm, mix_ref, bias_ref, gain_ref, shift_ref, *rest
):
    count = len(pieces)
    w_hbm = rest[:count]
    gu_ref, gv_ref, pack_ref = rest[-14:-11]
    d_ref, w_ref, cot_ref, low_at, turned_at, bias_at, b_acc, g_acc, s_acc, m_acc, sems = rest[-11:]
    turns = u_ref.shape[0] // PAIR
    step = pl.program_id(0)
    last = pl.num_programs(0) - 1

    def landing(k):
        slot, start, size = pieces[k]
        return w_ref.at[slot, :, pl.ds(start, size)]

    def cotangent(i, slot):
        return lax.dot_general(
            columns(d_ref, slice(i * PAIR, (i + 1) * PAIR)),
            columns(w_ref.at[slot], slice(None)),
            (((1,), (1,)), ((), ())),
            preferred_element_type=F32,
        )

    @pl.when(step == 0)
    def _():
        for k in range(count):
            if pieces[k][0] == 0:
                scatter_columns(w_hbm[k], landing(k), sems.at[k])
        scatter_columns(d_hbm, d_ref, sems.at[count])
        for k in range(count):
            if pieces[k][0] > 0:
                scatter_columns(w_hbm[k], landing(k), sems.at[k])
        for k in range(count):
            if pieces[k][0] == 0:
                await_all(landing(k), sems.at[k])
        await_all(d_ref, sems.at[count])
        cot_ref[0] = cotangent(0, 0)

    for k in range(count):
        if pieces[k][0] > 0:
            @pl.when(step == pieces[k][0] - 1)
            def _(k=k):
                await_all(landing(k), sems.at[k])

    for g in range(2):
        lower = lower_of(mix_ref[0, g].astype(F32))
        low_at[g] = lower.astype(BF16)
        turned_at[g] = lower.T.astype(BF16)
        bias_at[g] = upright(bias_ref[0, g : g + 1])
    b_acc[...] = jnp.zeros_like(b_acc)
    g_acc[...] = jnp.zeros_like(g_acc)
    s_acc[...] = jnp.zeros_like(s_acc)
    m_acc[...] = jnp.zeros_like(m_acc)
    for i in range(turns):
        if i + 1 < turns:
            cot_ref[(i + 1) % 2] = cotangent(i + 1, step)
        else:
            cot_ref[0] = cotangent(0, jnp.minimum(step + 1, last))
        for g in range(2):
            gain, shift = ROOT * gain_ref[0, g : g + 1], shift_ref[0, g : g + 1]
            rows = [slice(i * PAIR + h * BLK, i * PAIR + (h + 1) * BLK) for h in range(2)]
            kept, normed = [], []
            for at in rows:
                gated, slope = gelu_and_slope(v_ref[at, cols_of(g)].astype(F32))
                scaled, inverse = norm(gated)
                kept.append((scaled, inverse * slope))
                normed.append((scaled * gain + shift).astype(BF16))
            normed = jnp.concatenate(normed, axis=1)
            mixed = jnp.dot(low_at[g], normed, preferred_element_type=F32)
            d_mixed_b = []
            for h, at in enumerate(rows):
                upper, slope = gelu_and_slope(u_ref[at, cols_of(g)].astype(F32))
                cot = cot_ref[i % 2, h * BLK : (h + 1) * BLK, cols_of(g)]
                d_mixed = cot * upper
                d_mixed_b.append(d_mixed.astype(BF16))
                b_acc[g] += d_mixed
                gu_ref[at, cols_of(g)] = (
                    cot * slope * (mixed[:, cols_of(h)] + bias_at[g])
                ).astype(BF16)
            d_mixed_b = jnp.concatenate(d_mixed_b, axis=1)
            m_acc[g] += lax.dot_general(
                d_mixed_b, normed, (((1,), (1,)), ((), ())), preferred_element_type=F32
            )
            d_normed = jnp.dot(turned_at[g], d_mixed_b, preferred_element_type=F32)
            for h, at in enumerate(rows):
                scaled, scale = kept[h]
                dn = d_normed[:, cols_of(h)]
                weighted = dn * scaled
                g_acc[g] += jnp.sum(weighted.reshape(BLK // 8, 8, BLK), axis=0)
                s_acc[g] += jnp.sum(dn.reshape(BLK // 8, 8, BLK), axis=0)
                e = dn * gain
                mean_e = jnp.mean(e, axis=-1, keepdims=True)
                sum_es = jnp.sum(weighted * gain, axis=-1, keepdims=True)
                gv_ref[at, cols_of(g)] = (scale * (e - mean_e - scaled * sum_es)).astype(BF16)

    extra = []
    for g in range(2):
        extra.append(jnp.sum(b_acc[g].T, axis=0, keepdims=True))
        extra.append(ROOT * jnp.sum(g_acc[g], axis=0, keepdims=True))
        extra.append(jnp.sum(s_acc[g], axis=0, keepdims=True))
    row = lax.broadcasted_iota(jnp.int32, (BLK, BLK), 0)
    col = lax.broadcasted_iota(jnp.int32, (BLK, BLK), 1)
    extra.append(jnp.sum(jnp.where(row == col, m_acc[1], 0.0), axis=0, keepdims=True))
    both = jnp.where(row >= col, m_acc[0], m_acc[1].T)
    while len(extra) < SIDE:
        extra.append(jnp.zeros((1, BLK), F32))
    tiles = [both[k * SIDE : (k + 1) * SIDE] for k in range(BLK // SIDE)]
    tiles.append(jnp.concatenate(extra, axis=0))
    pack_ref[0] = jnp.concatenate(tiles, axis=1).astype(BF16)


def unpack_kernel(here, mine_ref, theirs_ref, gw_ref, gb_ref, gg_ref, gs_ref):
    count = mine_ref.shape[0]
    row = lax.broadcasted_iota(jnp.int32, (BLK, BLK), 0)
    col = lax.broadcasted_iota(jnp.int32, (BLK, BLK), 1)

    @pl.loop(0, count)
    def _(k):
        first = 2 * lax.rem(here[0] - k + count, count)
        for ref, core in ((mine_ref, here[1]), (theirs_ref, 1 - here[1])):
            pair = first + core
            x = ref[k].astype(F32)
            both = jnp.concatenate([x[:, cols_of(j)] for j in range(BLK // SIDE)], axis=0)
            vector = lambda j: x[j : j + 1, cols_of(BLK // SIDE)]
            gw_ref[2 * pair] = jnp.where(row >= col, both, 0.0)
            gw_ref[2 * pair + 1] = jnp.where(
                row > col, both.T, jnp.where(row == col, vector(6), 0.0)
            )
            for g in range(2):
                at = pl.ds(2 * pair + g, 1)
                gb_ref[at] = vector(3 * g)
                gg_ref[at] = vector(3 * g + 1)
                gs_ref[at] = vector(3 * g + 2)


def unpack(here, mine, theirs):
    groups = 4 * mine.shape[0]
    row = jax.ShapeDtypeStruct((groups, BLK), F32)
    vmem = pl.BlockSpec(memory_space=pltpu.VMEM)
    return pl.pallas_call(
        unpack_kernel,
        in_specs=[pl.BlockSpec(memory_space=pltpu.SMEM), vmem, vmem],
        out_specs=[vmem] * 4,
        out_shape=[jax.ShapeDtypeStruct((groups, BLK, BLK), F32), row, row, row],
        cost_estimate=pl.CostEstimate(flops=10**6, bytes_accessed=10**6, transcendentals=0),
        name="unpack",
    )(here, mine, theirs)


def join_kernel(a_hbm, b_hbm, out_hbm, a_ref, b_ref, out_ref, sems):
    count = a_hbm.shape[0]
    hbm = (a_hbm, b_hbm, out_hbm)
    vmem = (a_ref, b_ref, out_ref)
    read = lambda s, k: pltpu.make_async_copy(hbm[s].at[k], vmem[s].at[k], sems.at[s, k])
    write = lambda k: pltpu.make_async_copy(out_ref.at[k], out_hbm.at[k], sems.at[2, k])

    for k in range(count):
        read(0, k).start()
        read(1, k).start()

    @pl.loop(0, count)
    def _(k):
        read(0, k).wait()
        read(1, k).wait()
        out_ref[k] = (a_ref[k].astype(F32) + b_ref[k].astype(F32)).astype(BF16)
        write(k).start()

    for k in range(count):
        write(k).wait()


def join(a, b):
    n, rows, width = a.shape
    parts = (4 * n, rows // 4, width)
    hbm = pl.BlockSpec(memory_space=pl.ANY)
    return pl.pallas_call(
        join_kernel,
        in_specs=[hbm, hbm],
        out_specs=hbm,
        out_shape=jax.ShapeDtypeStruct(parts, BF16),
        scratch_shapes=[pltpu.VMEM(parts, BF16)] * 3 + [pltpu.SemaphoreType.DMA((3, 4 * n))],
        cost_estimate=pl.CostEstimate(
            flops=a.size, bytes_accessed=6 * a.size, transcendentals=0
        ),
        name="join",
    )(a.reshape(parts), b.reshape(parts)).reshape(a.shape)


def backward(here, weights, u, v, d, mix, bias, gain, shift):
    length, width = u.shape
    n = pairs = width // PAIR
    half = n // 2

    def pair_at(j, o):
        core = jnp.where(j < half, 1 - o[1], o[1])
        return lax.rem(o[0] + lax.rem(j, half), half) * 2 + core

    pieces = tuple((slot, start, w.shape[0]) for slot, start, w in weights)
    cur = lambda j, o: (0, pair_at(j, o))
    par = lambda j, o: (pair_at(j, o), 0, 0)
    mat = pl.BlockSpec((1, 2, BLK, BLK), lambda j, o: (pair_at(j, o), 0, 0, 0))
    tile = pl.BlockSpec((length, PAIR), cur)
    vec = pl.BlockSpec((1, 2, BLK), par)
    hbm = pl.BlockSpec(memory_space=pl.ANY)
    shapes = [
        jax.ShapeDtypeStruct((length, width), BF16),
        jax.ShapeDtypeStruct((length, width), BF16),
        jax.ShapeDtypeStruct((pairs, SIDE, PACK), BF16),
    ]
    return pl.pallas_call(
        functools.partial(backward_kernel, pieces),
        grid_spec=pltpu.PrefetchScalarGridSpec(
            num_scalar_prefetch=1,
            grid=(n,),
            in_specs=[
                tile,
                tile,
                hbm,
                mat,
                vec,
                vec,
                vec,
                *[hbm] * len(weights),
            ],
            out_specs=[
                tile,
                tile,
                pl.BlockSpec((1, SIDE, PACK), lambda j, o: (j, 0, 0)),
            ],
            scratch_shapes=[
                pltpu.VMEM((width // BLK, length, BLK), BF16),
                pltpu.VMEM((n, width // BLK, PAIR, BLK), BF16),
                pltpu.VMEM((2, PAIR, PAIR), F32),
                pltpu.VMEM((2, BLK, BLK), BF16),
                pltpu.VMEM((2, BLK, BLK), BF16),
                pltpu.VMEM((2, BLK, BLK), F32),
                pltpu.VMEM((2, BLK, BLK), F32),
                pltpu.VMEM((2, 8, BLK), F32),
                pltpu.VMEM((2, 8, BLK), F32),
                pltpu.VMEM((2, BLK, BLK), F32),
                pltpu.SemaphoreType.DMA((len(weights) + 1,)),
            ],
        ),
        out_shape=shapes,
        cost_estimate=pl.CostEstimate(
            flops=2 * n * PAIR * length * (width + 3 * BLK) * 2,
            bytes_accessed=length * width * 2 + n * PAIR * (8 * length + 2 * width),
            transcendentals=3 * n * PAIR * length,
        ),
        name="bwd",
    )(here, u, v, d, mix, bias, gain, shift, *[w for _, _, w in weights])


def hop(a, axis, size, by):
    return lax.ppermute(a, axis, [(i, (i + by) % size) for i in range(size)])


def total_of(parts):
    a, b, c, d = [p.astype(F32) for p in parts]
    return lax.optimization_barrier((a + c) + (b + d)).astype(BF16)


def added(a):
    return lax.optimization_barrier(jnp.sum(a.astype(F32), axis=0)).astype(BF16)


def spread(a, axes, count):
    return lax.all_to_all(jnp.broadcast_to(a[None], (count,) + a.shape), axes, 0, 0)


def on_device(u_pre, v_pre, d_out, w_mix, mix_bias, norm_gain, norm_shift, w_out, sizes=None):
    return everything(
        u_pre, v_pre, d_out, w_mix, mix_bias, norm_gain, norm_shift, w_out, sizes
    )


def everything(u_pre, v_pre, d_out, w_mix, mix_bias, norm_gain, norm_shift, w_out, sizes):
    nz, ny, nx, nc = sizes
    plane = nz * ny
    u, v, d = u_pre[0], v_pre[0], d_out[0]
    _, width = u.shape
    groups = w_mix.shape[0]
    pairs = groups // 2
    x, c = lax.axis_index("x"), lax.axis_index("c")
    here = jnp.stack([x, c]).astype(jnp.int32)

    swap = lambda a: hop(a, "c", nc, 1)
    half = w_out.shape[0] // 2
    own = swap(w_out)
    left = hop(w_out, "x", nx, 1)
    right = hop(w_out, "x", nx, -1)
    far0 = hop(left[:half], "x", nx, 1)
    far1 = hop(right[half:], "x", nx, -1)
    near = [swap(left), swap(right)]
    far = [swap(far0), swap(far1)]

    mix = w_mix.reshape(pairs, 2, BLK, BLK)
    bias = mix_bias.reshape(pairs, 2, BLK)
    gain = norm_gain.reshape(pairs, 2, BLK)
    shift = norm_shift.reshape(pairs, 2, BLK)

    common = (u, v, d, mix, bias, gain, shift)
    theirs = forward(here, True, *common)
    ours = forward(here, False, *common)
    traded = swap(theirs)
    joined = join(ours, traded)
    split = lax.all_to_all(joined.reshape(nx * plane, PAIR // plane, width), ("x", "z", "y"), 0, 0)

    weights = [
        (0, 0, own),
        (1, 0, near[1]),
        (2, 0, far[0]),
        (2, half, far[1]),
        (3, 0, near[0]),
        (4, 0, w_out),
        (5, 0, right),
        (6, 0, far0),
        (6, half, far1),
        (7, 0, left),
    ]
    grad_u, grad_v, packed = backward(here, weights, *common)

    mine = packed[nx:].astype(F32) + swap(packed[:nx]).astype(F32)
    mine = lax.optimization_barrier(mine).astype(BF16)
    arrived = [hop(mine[k], "x", nx, k) for k in range(1, nx)]
    ours = total_of([mine[0]] + arrived)
    for axis, size in (("y", ny), ("z", nz)):
        arrived = [hop(ours, axis, size, k) for k in range(1, size)]
        ours = total_of([ours] + arrived)
    rows = added(split)
    gathered = spread(rows, ("z", "y"), plane)
    ours = jnp.stack([ours] + [hop(ours, "x", nx, k) for k in range(1, nx)])
    others = swap(ours)
    grad_w, *vectors = unpack(here, ours, others)
    grad_w_out = gathered.reshape(PAIR, width).astype(F32)
    return (grad_u[None], grad_v[None], grad_w_out, grad_w, *vectors)


def solution(mesh):
    devices = mesh.devices.reshape(4, -1, *[mesh.devices.shape[1] // 2, 2])
    grid = Mesh(devices, ("z", "y", "x", "c"))
    big = P(("x", "c"), ("z", "y"), None)
    rows = P(("x", "c"), None)
    return jax.shard_map(
        functools.partial(on_device, sizes=devices.shape),
        mesh=grid,
        in_specs=(big, big, big, P(), P(), P(), P(), rows),
        out_specs=(big, big, rows, P(), P(), P(), P()),
        check_vma=False,
    )
```

profile of v0, /device:TPU:0, one launch (start us, length us, event | category | flops | bytes accessed | tf_op | source)
XLA Modules:
  0.0 174.1 jit_solution(3322217472613935514)
XLA Ops:
  0.6 0.7 pad_add_fusion.order.here
  1.3 13.1 %fwd.3 = bf16[4,256,2048]{2,1,0:T(8,128)(2,1)} custom-call(s32[2]{0:T(128)} %pad_add_fusion.order.here, bf16[1024,2048]{1,0:T(8,128)(2,1)} %bitcast.38, bf16[1024,2048]{1,0:T(8,128)(2,1)} %bitcast.41, bf16[1024,2048]{1,0:T(8,128)(2,1)} %bitcast.44, bf16[8,2,128,128]{3,2,1,0:T(8,128)(2,1)} %bitcast.47, f32[8,2,128]{2,1,0:T(2,128)} %bitcast.50, ...), custom_call_target="tpu_custom_call" | custom-call | flops 9126805504 | bytes 12582912 | tf_op jit(solution)/shard_map/fwd/pallas_call | solution.py:141
  14.4 0.1 collective-permute-start.9
  14.5 1.7 collective-permute-start.3
  16.2 1.6 collective-permute-start.1
  17.8 23.7 %collective-permute-done.3.rest_9_ = bf16[256,2048]{1,0:T(8,128)(2,1)S(1)} collective-permute-done((bf16[256,2048]{1,0:T(8,128)(2,1)}, bf16[256,2048]{1,0:T(8,128)(2,1)S(1)}, u32[]{:S(2)}, u32[]{:S(2)}) %collective-permute-start.3) | collective-permute-done | bytes 1048608 | tf_op jit(solution)/shard_map/ppermute | solution.py:428
  41.6 0.5 collective-permute-start.4
  42.1 2.9 %collective-permute-start.6 = (bf16[128,2048]{1,0:T(8,128)(2,1)S(1)}, bf16[128,2048]{1,0:T(8,128)(2,1)}, u32[]{:S(2)}, u32[]{:S(2)}) collective-permute-start(bf16[128,2048]{1,0:T(8,128)(2,1)S(1)} %slice.33), channel_id=1, source_target_pairs={{0,6},{2,0},{4,2},{6,4},{1,7},{3,1},{5,3},{7,5},{8,14},{10,8},{12,... | collective-permute-start | bytes 1572872 | tf_op jit(solution)/shard_map/ppermute | solution.py:428
  45.0 0.5 collective-permute-start.8
  45.5 13.1 %fwd.2 = bf16[4,256,2048]{2,1,0:T(8,128)(2,1)} custom-call(s32[2]{0:T(128)} %pad_add_fusion.order.here, bf16[1024,2048]{1,0:T(8,128)(2,1)} %bitcast.39, bf16[1024,2048]{1,0:T(8,128)(2,1)} %bitcast.42, bf16[1024,2048]{1,0:T(8,128)(2,1)} %bitcast.45, bf16[8,2,128,128]{3,2,1,0:T(8,128)(2,1)} %bitcast.48, f32[8,2,128]{2,1,0:T(2,128)} %bitcast.51, ...), custom_call_target="tpu_custom_call" | custom-call | flops 9126805504 | bytes 12582912 | tf_op jit(solution)/shard_map/fwd/pallas_call | solution.py:141
  58.7 5.6 %join.1 = bf16[16,64,2048]{2,1,0:T(8,128)(2,1)} custom-call(bf16[16,64,2048]{2,1,0:T(8,128)(2,1)} %bitcast.33, bf16[16,64,2048]{2,1,0:T(8,128)(2,1)} %bitcast.12.b_hbm), custom_call_target="tpu_custom_call" | custom-call | flops 2097152 | bytes 12582912 | tf_op jit(solution)/shard_map/join/pallas_call | solution.py:349
  64.3 9.4 %all-to-all-start = ((bf16[64,16,2048]{2,1,0:T(8,128)(2,1)}), bf16[64,16,2048]{2,1,0:T(8,128)(2,1)}, u32[]{:S(2)}, u32[]{:S(2)}) async-start(bf16[64,16,2048]{2,1,0:T(8,128)(2,1)} %bitcast.32), calls=%async_computation | async-start | bytes 8388608 | tf_op jit(solution)/shard_map/all_to_all | solution.py:480
  73.6 0.1 collective-permute-start.5
  73.8 0.5 collective-permute-start.7
  74.2 1.6 collective-permute-done.5.rest_2_
  75.9 0.7 collective-permute-done.7.rest_3_
  76.6 0.1 copy-done.4
  76.7 0.7 copy-done.5
  77.4 28.6 %bwd.1 = (bf16[1024,2048]{1,0:T(8,128)(2,1)}, bf16[1024,2048]{1,0:T(8,128)(2,1)}, bf16[8,16,1152]{2,1,0:T(8,128)(2,1)}) custom-call(s32[2]{0:T(128)} %pad_add_fusion.order.here, bf16[1024,2048]{1,0:T(8,128)(2,1)} %bitcast.40, bf16[1024,2048]{1,0:T(8,128)(2,1)} %bitcast.43, bf16[1024,2048]{1,0:T(8,128)(2,1)} %bitcast.46, bf16[8,2,128,128]{3,2,1,0:T(8,128)(2,1)} %bitcast.49, ...), custom_call_target="tpu_custom_call" | custom-call | flops 20401094656 | bytes 29360128 | tf_op jit(solution)/shard_map/bwd/pallas_call | solution.py:383
  106.0 0.9 slice.27
  106.9 0.2 collective-permute-start.10
  107.1 1.2 collective-permute-done.10
  108.4 1.0 convert_add_fusion
  109.3 3.0 %collective-permute-start.13 = (bf16[16,1152]{1,0:T(8,128)(2,1)S(1)}, bf16[16,1152]{1,0:T(8,128)(2,1)S(1)}, u32[]{:S(2)}, u32[]{:S(2)}) collective-permute-start(bf16[16,1152]{1,0:T(8,128)(2,1)S(1)} %get-tuple-element.23), channel_id=1, source_target_pairs={{0,6},{2,0},{4,2},{6,4},{1,7},{3,1},{5,3},{7,5},{8,14},{10,8},{12,... | collective-permute-start | bytes 110600 | tf_op jit(solution)/shard_map/ppermute | solution.py:428
  112.3 2.2 %collective-permute-start.11 = (bf16[16,1152]{1,0:T(8,128)(2,1)S(1)}, bf16[16,1152]{1,0:T(8,128)(2,1)S(1)}, u32[]{:S(2)}, u32[]{:S(2)}) collective-permute-start(bf16[16,1152]{1,0:T(8,128)(2,1)S(1)} %get-tuple-element.21), channel_id=1, source_target_pairs={{0,4},{2,6},{4,0},{6,2},{1,5},{3,7},{5,1},{7,3},{8,12},{10,14},{12... | collective-permute-start | bytes 110600 | tf_op jit(solution)/shard_map/ppermute | solution.py:428
  114.5 10.5 %collective-permute-done.13 = bf16[16,1152]{1,0:T(8,128)(2,1)S(1)} collective-permute-done((bf16[16,1152]{1,0:T(8,128)(2,1)S(1)}, bf16[16,1152]{1,0:T(8,128)(2,1)S(1)}, u32[]{:S(2)}, u32[]{:S(2)}) %collective-permute-start.13) | collective-permute-done | bytes 36896 | tf_op jit(solution)/shard_map/ppermute | solution.py:428
  125.0 1.8 %collective-permute-done.12 = bf16[16,1152]{1,0:T(8,128)(2,1)S(1)} collective-permute-done((bf16[16,1152]{1,0:T(8,128)(2,1)S(1)}, bf16[16,1152]{1,0:T(8,128)(2,1)S(1)}, u32[]{:S(2)}, u32[]{:S(2)}) %collective-permute-start.12) | collective-permute-done | bytes 36896 | tf_op jit(solution)/shard_map/ppermute | solution.py:428
  126.9 1.9 %collective-permute-start.16 = (bf16[16,1152]{1,0:T(8,128)(2,1)S(1)}, bf16[16,1152]{1,0:T(8,128)(2,1)S(1)}, u32[]{:S(2)}, u32[]{:S(2)}) collective-permute-start(bf16[16,1152]{1,0:T(8,128)(2,1)S(1)} %fusion), channel_id=1, source_target_pairs={{0,24},{8,0},{16,8},{24,16},{1,25},{9,1},{17,9},{25,17},{2,26},{10... | collective-permute-start | bytes 110600 | tf_op jit(solution)/shard_map/ppermute | solution.py:428
  128.7 0.2 collective-permute-start.15
  129.0 2.9 %collective-permute-start.14 = (bf16[16,1152]{1,0:T(8,128)(2,1)S(1)}, bf16[16,1152]{1,0:T(8,128)(2,1)S(1)}, u32[]{:S(2)}, u32[]{:S(2)}) collective-permute-start(bf16[16,1152]{1,0:T(8,128)(2,1)S(1)} %fusion), channel_id=1, source_target_pairs={{0,16},{8,24},{16,0},{24,8},{1,17},{9,25},{17,1},{25,9},{2,18},{10... | collective-permute-start | bytes 110600 | tf_op jit(solution)/shard_map/ppermute | solution.py:428
  131.9 2.8 %convert_reduce_fusion = bf16[16,2048]{1,0:T(8,128)(2,1)S(1)} fusion(bf16[64,16,2048]{2,1,0:T(8,128)(2,1)} %all-to-all-done), kind=kLoop, calls=%fused_computation | loop fusion | flops 4161536 | bytes 4259840 | tf_op jit(solution)/shard_map/reduce_sum | solution.py:437
  134.7 1.1 broadcast_in_dim.14
  135.8 6.6 %all-to-all-start.1 = ((bf16[16,16,2048]{2,1,0:T(8,128)(2,1)}), bf16[16,16,2048]{2,1,0:T(8,128)(2,1)S(1)}, u32[]{:S(2)}, u32[]{:S(2)}) async-start(bf16[16,16,2048]{2,1,0:T(8,128)(2,1)} %broadcast_in_dim.14), calls=%async_computation.1 | async-start | bytes 2097152 | tf_op jit(solution)/shard_map/all_to_all | solution.py:441
  142.4 3.2 %collective-permute-start.19 = (bf16[16,1152]{1,0:T(8,128)(2,1)S(1)}, bf16[16,1152]{1,0:T(8,128)(2,1)S(1)}, u32[]{:S(2)}, u32[]{:S(2)}) collective-permute-start(bf16[16,1152]{1,0:T(8,128)(2,1)S(1)} %add_add_fusion.1), channel_id=1, source_target_pairs={{0,96},{32,0},{64,32},{96,64},{1,97},{33,1},{65,33},{97,65},{2,98}... | collective-permute-start | bytes 110600 | tf_op jit(solution)/shard_map/ppermute | solution.py:428
  145.6 2.3 %collective-permute-start.17 = (bf16[16,1152]{1,0:T(8,128)(2,1)S(1)}, bf16[16,1152]{1,0:T(8,128)(2,1)S(1)}, u32[]{:S(2)}, u32[]{:S(2)}) collective-permute-start(bf16[16,1152]{1,0:T(8,128)(2,1)S(1)} %add_add_fusion.1), channel_id=1, source_target_pairs={{0,64},{32,96},{64,0},{96,32},{1,65},{33,97},{65,1},{97,33},{2,66}... | collective-permute-start | bytes 110600 | tf_op jit(solution)/shard_map/ppermute | solution.py:428
  147.9 7.8 %collective-permute-done.19 = bf16[16,1152]{1,0:T(8,128)(2,1)S(1)} collective-permute-done((bf16[16,1152]{1,0:T(8,128)(2,1)S(1)}, bf16[16,1152]{1,0:T(8,128)(2,1)S(1)}, u32[]{:S(2)}, u32[]{:S(2)}) %collective-permute-start.19) | collective-permute-done | bytes 36896 | tf_op jit(solution)/shard_map/ppermute | solution.py:428
  155.7 1.0 collective-permute-done.18
  156.7 5.3 %collective-permute-start.22 = (bf16[16,1152]{1,0:T(8,128)(2,1)S(1)}, bf16[16,1152]{1,0:T(8,128)(2,1)S(1)}, u32[]{:S(2)}, u32[]{:S(2)}) collective-permute-start(bf16[16,1152]{1,0:T(8,128)(2,1)S(1)} %add_add_fusion), channel_id=1, source_target_pairs={{0,6},{2,0},{4,2},{6,4},{1,7},{3,1},{5,3},{7,5},{8,14},{10,8},{12,... | collective-permute-start | bytes 110600 | tf_op jit(solution)/shard_map/ppermute | solution.py:428
  162.0 0.4 collective-permute-start.21
  162.4 0.5 collective-permute-start.20
  162.9 0.7 collective-permute-done.22
  163.6 3.9 %collective-permute-done.21 = bf16[16,1152]{1,0:T(8,128)(2,1)S(1)} collective-permute-done((bf16[16,1152]{1,0:T(8,128)(2,1)S(1)}, bf16[16,1152]{1,0:T(8,128)(2,1)S(1)}, u32[]{:S(2)}, u32[]{:S(2)}) %collective-permute-start.21) | collective-permute-done | bytes 36896 | tf_op jit(solution)/shard_map/ppermute | solution.py:428
  167.5 0.4 collective-permute-done.20
  167.9 0.1 collective-permute-start.23
  168.0 1.4 collective-permute-done.23.theirs_ref
  169.3 0.7 copy-done.3
  170.0 2.4 %unpack.1 = (f32[16,128,128]{2,1,0:T(8,128)}, f32[16,128]{1,0:T(8,128)}, f32[16,128]{1,0:T(8,128)}, f32[16,128]{1,0:T(8,128)}) custom-call(s32[2]{0:T(128)} %pad_add_fusion.order.here, bf16[4,16,1152]{2,1,0:T(8,128)(2,1)} %copy-done, bf16[4,16,1152]{2,1,0:T(8,128)(2,1)} %copy-done.3), custom_call_target="tpu_custom_call" | custom-call | flops 1000000 | bytes 1000000 | tf_op jit(solution)/shard_map/unpack/pallas_call | solution.py:313
  172.4 1.6 bitcast_convert_fusion
  (34 shorter events, 0.3 us)
Async XLA Ops:
  14.4 30.6 %collective-permute-start.9 = (bf16[4,256,2048]{2,1,0:T(8,128)(2,1)}, bf16[4,256,2048]{2,1,0:T(8,128)(2,1)}, u32[]{:S(2)}, u32[]{:S(2)}) collective-permute-start(bf16[4,256,2048]{2,1,0:T(8,128)(2,1)} %fwd.3), channel_id=1, source_target_pairs={{0,1},{1,0},{2,3},{3,2},{4,5},{5,4},{6,7},{7,6},{8,9},{9,8},{10,11... | collective-permute-start | bytes 12582920 | tf_op jit(solution)/shard_map/ppermute | solution.py:428
  14.5 27.0 %collective-permute-start.3 = (bf16[256,2048]{1,0:T(8,128)(2,1)}, bf16[256,2048]{1,0:T(8,128)(2,1)S(1)}, u32[]{:S(2)}, u32[]{:S(2)}) collective-permute-start(bf16[256,2048]{1,0:T(8,128)(2,1)} %rest_5_.1), channel_id=1, source_target_pairs={{0,2},{2,4},{4,6},{6,0},{1,3},{3,5},{5,7},{7,1},{8,10},{10,12},{12... | collective-permute-start | bytes 3145736 | tf_op jit(solution)/shard_map/ppermute | solution.py:428
  16.2 25.8 %collective-permute-start.1 = (bf16[256,2048]{1,0:T(8,128)(2,1)}, bf16[256,2048]{1,0:T(8,128)(2,1)S(1)}, u32[]{:S(2)}, u32[]{:S(2)}) collective-permute-start(bf16[256,2048]{1,0:T(8,128)(2,1)} %rest_5_.1), channel_id=1, source_target_pairs={{0,6},{2,0},{4,2},{6,4},{1,7},{3,1},{5,3},{7,5},{8,14},{10,8},{12,... | collective-permute-start | bytes 3145736 | tf_op jit(solution)/shard_map/ppermute | solution.py:428
  17.8 56.4 %collective-permute-start = (bf16[256,2048]{1,0:T(8,128)(2,1)}, bf16[256,2048]{1,0:T(8,128)(2,1)}, u32[]{:S(2)}, u32[]{:S(2)}) collective-permute-start(bf16[256,2048]{1,0:T(8,128)(2,1)} %rest_5_.1), channel_id=1, source_target_pairs={{0,1},{1,0},{2,3},{3,2},{4,5},{5,4},{6,7},{7,6},{8,9},{9,8},{10,11... | collective-permute-start | bytes 3145736 | tf_op jit(solution)/shard_map/ppermute | solution.py:428
  41.5 17.1 %copy-start.1 = (bf16[256,2048]{1,0:T(8,128)(2,1)}, bf16[256,2048]{1,0:T(8,128)(2,1)S(1)}, u32[]{:S(2)}) copy-start(bf16[256,2048]{1,0:T(8,128)(2,1)S(1)} %collective-permute-done.3.rest_9_) | copy-start | bytes 3145732
  41.6 32.1 %collective-permute-start.4 = (bf16[128,2048]{1,0:T(8,128)(2,1)S(1)}, bf16[128,2048]{1,0:T(8,128)(2,1)}, u32[]{:S(2)}, u32[]{:S(2)}) collective-permute-start(bf16[128,2048]{1,0:T(8,128)(2,1)S(1)} %slice.32), channel_id=1, source_target_pairs={{0,2},{2,4},{4,6},{6,0},{1,3},{3,5},{5,7},{7,1},{8,10},{10,12},{12... | collective-permute-start | bytes 1572872 | tf_op jit(solution)/shard_map/ppermute | solution.py:428
  42.0 16.6 %copy-start.2 = (bf16[256,2048]{1,0:T(8,128)(2,1)}, bf16[256,2048]{1,0:T(8,128)(2,1)S(1)}, u32[]{:S(2)}) copy-start(bf16[256,2048]{1,0:T(8,128)(2,1)S(1)} %collective-permute-done.1.rest_6_) | copy-start | bytes 3145732
  42.1 31.7 %collective-permute-start.6 = (bf16[128,2048]{1,0:T(8,128)(2,1)S(1)}, bf16[128,2048]{1,0:T(8,128)(2,1)}, u32[]{:S(2)}, u32[]{:S(2)}) collective-permute-start(bf16[128,2048]{1,0:T(8,128)(2,1)S(1)} %slice.33), channel_id=1, source_target_pairs={{0,6},{2,0},{4,2},{6,4},{1,7},{3,1},{5,3},{7,5},{8,14},{10,8},{12,... | collective-permute-start | bytes 1572872 | tf_op jit(solution)/shard_map/ppermute | solution.py:428
  45.0 29.3 %collective-permute-start.2 = (bf16[256,2048]{1,0:T(8,128)(2,1)S(1)}, bf16[256,2048]{1,0:T(8,128)(2,1)}, u32[]{:S(2)}, u32[]{:S(2)}) collective-permute-start(bf16[256,2048]{1,0:T(8,128)(2,1)S(1)} %collective-permute-done.1.rest_6_), channel_id=1, source_target_pairs={{0,1},{1,0},{2,3},{3,2},{4,5},{5,4},{6,7},{7,6},{8,9},{9,8},{10,11... | collective-permute-start | bytes 3145736 | tf_op jit(solution)/shard_map/ppermute | solution.py:428
  45.0 31.6 %collective-permute-start.8 = (bf16[256,2048]{1,0:T(8,128)(2,1)S(1)}, bf16[256,2048]{1,0:T(8,128)(2,1)}, u32[]{:S(2)}, u32[]{:S(2)}) collective-permute-start(bf16[256,2048]{1,0:T(8,128)(2,1)S(1)} %collective-permute-done.3.rest_9_), channel_id=1, source_target_pairs={{0,1},{1,0},{2,3},{3,2},{4,5},{5,4},{6,7},{7,6},{8,9},{9,8},{10,11... | collective-permute-start | bytes 3145736 | tf_op jit(solution)/shard_map/ppermute | solution.py:428
  64.3 67.6 %all-to-all-start = ((bf16[64,16,2048]{2,1,0:T(8,128)(2,1)}), bf16[64,16,2048]{2,1,0:T(8,128)(2,1)}, u32[]{:S(2)}, u32[]{:S(2)}) async-start(bf16[64,16,2048]{2,1,0:T(8,128)(2,1)} %bitcast.32), calls=%async_computation | async-start | bytes 8388608 | tf_op jit(solution)/shard_map/all_to_all | solution.py:480
  73.6 2.2 %collective-permute-start.5 = (bf16[128,2048]{1,0:T(8,128)(2,1)}, bf16[128,2048]{1,0:T(8,128)(2,1)S(1)}, u32[]{:S(2)}, u32[]{:S(2)}) collective-permute-start(bf16[128,2048]{1,0:T(8,128)(2,1)} %collective-permute-done.4.rest_7_), channel_id=1, source_target_pairs={{0,1},{1,0},{2,3},{3,2},{4,5},{5,4},{6,7},{7,6},{8,9},{9,8},{10,11... | collective-permute-start | bytes 1572872 | tf_op jit(solution)/shard_map/ppermute | solution.py:428
  73.8 2.8 %collective-permute-start.7 = (bf16[128,2048]{1,0:T(8,128)(2,1)}, bf16[128,2048]{1,0:T(8,128)(2,1)S(1)}, u32[]{:S(2)}, u32[]{:S(2)}) collective-permute-start(bf16[128,2048]{1,0:T(8,128)(2,1)} %collective-permute-done.6.rest_8_), channel_id=1, source_target_pairs={{0,1},{1,0},{2,3},{3,2},{4,5},{5,4},{6,7},{7,6},{8,9},{9,8},{10,11... | collective-permute-start | bytes 1572872 | tf_op jit(solution)/shard_map/ppermute | solution.py:428
  75.8 0.8 copy-start.4
  76.6 0.8 copy-start.5
  106.9 1.5 collective-permute-start.10
  109.3 15.7 %collective-permute-start.13 = (bf16[16,1152]{1,0:T(8,128)(2,1)S(1)}, bf16[16,1152]{1,0:T(8,128)(2,1)S(1)}, u32[]{:S(2)}, u32[]{:S(2)}) collective-permute-start(bf16[16,1152]{1,0:T(8,128)(2,1)S(1)} %get-tuple-element.23), channel_id=1, source_target_pairs={{0,6},{2,0},{4,2},{6,4},{1,7},{3,1},{5,3},{7,5},{8,14},{10,8},{12,... | collective-permute-start | bytes 110600 | tf_op jit(solution)/shard_map/ppermute | solution.py:428
  112.3 14.5 %collective-permute-start.12 = (bf16[16,1152]{1,0:T(8,128)(2,1)S(1)}, bf16[16,1152]{1,0:T(8,128)(2,1)S(1)}, u32[]{:S(2)}, u32[]{:S(2)}) collective-permute-start(bf16[16,1152]{1,0:T(8,128)(2,1)S(1)} %get-tuple-element.22), channel_id=1, source_target_pairs={{0,2},{2,4},{4,6},{6,0},{1,3},{3,5},{5,7},{7,1},{8,10},{10,12},{12... | collective-permute-start | bytes 110600 | tf_op jit(solution)/shard_map/ppermute | solution.py:428
  112.3 14.5 %collective-permute-start.11 = (bf16[16,1152]{1,0:T(8,128)(2,1)S(1)}, bf16[16,1152]{1,0:T(8,128)(2,1)S(1)}, u32[]{:S(2)}, u32[]{:S(2)}) collective-permute-start(bf16[16,1152]{1,0:T(8,128)(2,1)S(1)} %get-tuple-element.21), channel_id=1, source_target_pairs={{0,4},{2,6},{4,0},{6,2},{1,5},{3,7},{5,1},{7,3},{8,12},{10,14},{12... | collective-permute-start | bytes 110600 | tf_op jit(solution)/shard_map/ppermute | solution.py:428
  126.9 15.5 %collective-permute-start.16 = (bf16[16,1152]{1,0:T(8,128)(2,1)S(1)}, bf16[16,1152]{1,0:T(8,128)(2,1)S(1)}, u32[]{:S(2)}, u32[]{:S(2)}) collective-permute-start(bf16[16,1152]{1,0:T(8,128)(2,1)S(1)} %fusion), channel_id=1, source_target_pairs={{0,24},{8,0},{16,8},{24,16},{1,25},{9,1},{17,9},{25,17},{2,26},{10... | collective-permute-start | bytes 110600 | tf_op jit(solution)/shard_map/ppermute | solution.py:428
  128.7 13.6 %collective-permute-start.15 = (bf16[16,1152]{1,0:T(8,128)(2,1)S(1)}, bf16[16,1152]{1,0:T(8,128)(2,1)S(1)}, u32[]{:S(2)}, u32[]{:S(2)}) collective-permute-start(bf16[16,1152]{1,0:T(8,128)(2,1)S(1)} %fusion), channel_id=1, source_target_pairs={{0,8},{8,16},{16,24},{24,0},{1,9},{9,17},{17,25},{25,1},{2,10},{10... | collective-permute-start | bytes 110600 | tf_op jit(solution)/shard_map/ppermute | solution.py:428
  129.0 13.4 %collective-permute-start.14 = (bf16[16,1152]{1,0:T(8,128)(2,1)S(1)}, bf16[16,1152]{1,0:T(8,128)(2,1)S(1)}, u32[]{:S(2)}, u32[]{:S(2)}) collective-permute-start(bf16[16,1152]{1,0:T(8,128)(2,1)S(1)} %fusion), channel_id=1, source_target_pairs={{0,16},{8,24},{16,0},{24,8},{1,17},{9,25},{17,1},{25,9},{2,18},{10... | collective-permute-start | bytes 110600 | tf_op jit(solution)/shard_map/ppermute | solution.py:428
  135.8 36.7 %all-to-all-start.1 = ((bf16[16,16,2048]{2,1,0:T(8,128)(2,1)}), bf16[16,16,2048]{2,1,0:T(8,128)(2,1)S(1)}, u32[]{:S(2)}, u32[]{:S(2)}) async-start(bf16[16,16,2048]{2,1,0:T(8,128)(2,1)} %broadcast_in_dim.14), calls=%async_computation.1 | async-start | bytes 2097152 | tf_op jit(solution)/shard_map/all_to_all | solution.py:441
  142.4 13.3 %collective-permute-start.19 = (bf16[16,1152]{1,0:T(8,128)(2,1)S(1)}, bf16[16,1152]{1,0:T(8,128)(2,1)S(1)}, u32[]{:S(2)}, u32[]{:S(2)}) collective-permute-start(bf16[16,1152]{1,0:T(8,128)(2,1)S(1)} %add_add_fusion.1), channel_id=1, source_target_pairs={{0,96},{32,0},{64,32},{96,64},{1,97},{33,1},{65,33},{97,65},{2,98}... | collective-permute-start | bytes 110600 | tf_op jit(solution)/shard_map/ppermute | solution.py:428
  145.6 11.1 %collective-permute-start.18 = (bf16[16,1152]{1,0:T(8,128)(2,1)S(1)}, bf16[16,1152]{1,0:T(8,128)(2,1)S(1)}, u32[]{:S(2)}, u32[]{:S(2)}) collective-permute-start(bf16[16,1152]{1,0:T(8,128)(2,1)S(1)} %add_add_fusion.1), channel_id=1, source_target_pairs={{0,32},{32,64},{64,96},{96,0},{1,33},{33,65},{65,97},{97,1},{2,34}... | collective-permute-start | bytes 110600 | tf_op jit(solution)/shard_map/ppermute | solution.py:428
  145.6 11.1 %collective-permute-start.17 = (bf16[16,1152]{1,0:T(8,128)(2,1)S(1)}, bf16[16,1152]{1,0:T(8,128)(2,1)S(1)}, u32[]{:S(2)}, u32[]{:S(2)}) collective-permute-start(bf16[16,1152]{1,0:T(8,128)(2,1)S(1)} %add_add_fusion.1), channel_id=1, source_target_pairs={{0,64},{32,96},{64,0},{96,32},{1,65},{33,97},{65,1},{97,33},{2,66}... | collective-permute-start | bytes 110600 | tf_op jit(solution)/shard_map/ppermute | solution.py:428
  156.7 6.9 %collective-permute-start.22 = (bf16[16,1152]{1,0:T(8,128)(2,1)S(1)}, bf16[16,1152]{1,0:T(8,128)(2,1)S(1)}, u32[]{:S(2)}, u32[]{:S(2)}) collective-permute-start(bf16[16,1152]{1,0:T(8,128)(2,1)S(1)} %add_add_fusion), channel_id=1, source_target_pairs={{0,6},{2,0},{4,2},{6,4},{1,7},{3,1},{5,3},{7,5},{8,14},{10,8},{12,... | collective-permute-start | bytes 110600 | tf_op jit(solution)/shard_map/ppermute | solution.py:428
  162.0 5.5 %collective-permute-start.21 = (bf16[16,1152]{1,0:T(8,128)(2,1)S(1)}, bf16[16,1152]{1,0:T(8,128)(2,1)S(1)}, u32[]{:S(2)}, u32[]{:S(2)}) collective-permute-start(bf16[16,1152]{1,0:T(8,128)(2,1)S(1)} %add_add_fusion), channel_id=1, source_target_pairs={{0,4},{2,6},{4,0},{6,2},{1,5},{3,7},{5,1},{7,3},{8,12},{10,14},{12... | collective-permute-start | bytes 110600 | tf_op jit(solution)/shard_map/ppermute | solution.py:428
  162.4 5.4 %collective-permute-start.20 = (bf16[16,1152]{1,0:T(8,128)(2,1)S(1)}, bf16[16,1152]{1,0:T(8,128)(2,1)S(1)}, u32[]{:S(2)}, u32[]{:S(2)}) collective-permute-start(bf16[16,1152]{1,0:T(8,128)(2,1)S(1)} %add_add_fusion), channel_id=1, source_target_pairs={{0,2},{2,4},{4,6},{6,0},{1,3},{3,5},{5,7},{7,1},{8,10},{10,12},{12... | collective-permute-start | bytes 110600 | tf_op jit(solution)/shard_map/ppermute | solution.py:428
  167.9 1.5 copy-start
  167.9 1.5 collective-permute-start.23
  169.3 0.7 copy-start.3
where the time goes:
time: 176 us; the launch traced here: 174 us
  Pallas kernels  62.9 us (36%)
  waiting for transfers between devices  54.6 us (31%)
  starting transfers between devices  46 us (26%)
  other arithmetic  6.17 us (4%)
  local copies, waits for them, and re-layouts  3.55 us (2%)
    ppermute x24, waiting for transfers between devices, hop(): return lax.ppermute(a, axis, [(i, (i + by) % size) for i in range(size)])  54.6 us
    ppermute x24, starting transfers between devices, hop(): return lax.ppermute(a, axis, [(i, (i + by) % size) for i in range(size)])  30.1 us
    pallas_call x1, Pallas kernels, backward(): pl.pallas_call(functools.partial(backward_kernel, pieces), grid_spec=pltp...  28.6 us
    pallas_call x2, Pallas kernels, forward(): pl.pallas_call(forward_kernel, grid_spec=pltpu.PrefetchScalarGridSpec(num...  26.2 us
    all_to_all x1, starting transfers between devices, everything(): lax.all_to_all(joined.reshape(nx * plane, PAIR // plane, width), ('x', 'z...  9.38 us
    all_to_all x1, starting transfers between devices, spread(): lax.all_to_all(jnp.broadcast_to(a[None], (count,) + a.shape), axes, 0, 0)  6.57 us
    pallas_call x1, Pallas kernels, join(): pl.pallas_call(join_kernel, in_specs=[hbm, hbm], out_specs=hbm, out_shape...  5.59 us
  transfers between devices with their start and end apart: 26, of which 12 were waited for; matrix products, arithmetic and copies ran while one was open for 3% of the time, Pallas kernels for 29%

commit v1 on v0

--- a/solution.py
+++ b/solution.py
@@ -428,17 +428,57 @@
     return lax.ppermute(a, axis, [(i, (i + by) % size) for i in range(size)])
 
 
+def row_sum_kernel(x_hbm, out_hbm, x_ref, acc_ref, row_ref, in_sems, out_sems):
+    count, each = x_ref.shape[:2]
+    copies = out_hbm.shape[0]
+    read = lambda k: pltpu.make_async_copy(
+        x_hbm.at[pl.ds(k * each, each)], x_ref.at[k], in_sems.at[k]
+    )
+    write = lambda k: pltpu.make_async_copy(row_ref, out_hbm.at[k], out_sems.at[k])
+
+    for k in range(count):
+        read(k).start()
+    acc_ref[...] = jnp.zeros_like(acc_ref)
+
+    @pl.loop(0, count)
+    def _(k):
+        read(k).wait()
+        total = x_ref[k, 0].astype(F32)
+        for r in range(1, each):
+            total = total + x_ref[k, r].astype(F32)
+        acc_ref[...] += total
+
+    row_ref[...] = acc_ref[...].astype(BF16)
+    for k in range(copies):
+        write(k).start()
+    for k in range(copies):
+        write(k).wait()
+
+
+def row_sum(x, copies):
+    n, rows, width = x.shape
+    count = 16
+    hbm = pl.BlockSpec(memory_space=pl.ANY)
+    return pl.pallas_call(
+        row_sum_kernel,
+        in_specs=[hbm],
+        out_specs=hbm,
+        out_shape=jax.ShapeDtypeStruct((copies, rows, width), BF16),
+        scratch_shapes=[
+            pltpu.VMEM((count, n // count, rows, width), BF16),
+            pltpu.VMEM((rows, width), F32),
+            pltpu.VMEM((rows, width), BF16),
+            pltpu.SemaphoreType.DMA((count,)),
+            pltpu.SemaphoreType.DMA((copies,)),
+        ],
+        cost_estimate=pl.CostEstimate(flops=x.size, bytes_accessed=3 * x.size, transcendentals=0),
+        name="row_sum",
+    )(x)
+
+
 def total_of(parts):
     a, b, c, d = [p.astype(F32) for p in parts]
     return lax.optimization_barrier((a + c) + (b + d)).astype(BF16)
-
-
-def added(a):
-    return lax.optimization_barrier(jnp.sum(a.astype(F32), axis=0)).astype(BF16)
-
-
-def spread(a, axes, count):
-    return lax.all_to_all(jnp.broadcast_to(a[None], (count,) + a.shape), axes, 0, 0)
 
 
 def on_device(u_pre, v_pre, d_out, w_mix, mix_bias, norm_gain, norm_shift, w_out, sizes=None):
@@ -500,8 +540,8 @@
     for axis, size in (("y", ny), ("z", nz)):
         arrived = [hop(ours, axis, size, k) for k in range(1, size)]
         ours = total_of([ours] + arrived)
-    rows = added(split)
-    gathered = spread(rows, ("z", "y"), plane)
+    rows = row_sum(split, plane)
+    gathered = lax.all_to_all(rows, ("z", "y"), 0, 0)
     ours = jnp.stack([ours] + [hop(ours, "x", nx, k) for k in range(1, nx)])
     others = swap(ours)
     grad_w, *vectors = unpack(here, ours, others)

time: 176 us -> 175 us (level)
  Pallas kernels: 62.9 us -> 66.3 us
  other arithmetic: 6.17 us -> 3.34 us
    pallas_call x0 -> x1, Pallas kernels: none -> 3.41 us  [row_sum(): pl.pallas_call(row_sum_kernel, in_specs=[hbm], out_specs=hbm, out_shape=j...]
    reduce_sum x1 -> x0, other arithmetic: 2.82 us -> none  [added(): return lax.optimization_barrier(jnp.sum(a.astype(F32), axis=0)).astype(BF16)]
  transfers between devices with their start and end apart: 26 -> 26, of which waited for: 12 -> 12; matrix products, arithmetic and copies ran while one was open for 3% -> 1% of each run, Pallas kernels for 29% -> 31%
where the time goes in v1:
time: 175 us; the launch traced here: 174 us
  Pallas kernels  66.3 us (38%)
  waiting for transfers between devices  54.6 us (31%)
  starting transfers between devices  46 us (26%)
  other arithmetic  3.34 us (2%)
  local copies, waits for them, and re-layouts  2.46 us (1%)
    ppermute x24, waiting for transfers between devices, hop(): return lax.ppermute(a, axis, [(i, (i + by) % size) for i in range(size)])  54.6 us
    ppermute x24, starting transfers between devices, hop(): return lax.ppermute(a, axis, [(i, (i + by) % size) for i in range(size)])  30.1 us
    pallas_call x1, Pallas kernels, backward(): pl.pallas_call(functools.partial(backward_kernel, pieces), grid_spec=pltp...  28.6 us
    pallas_call x2, Pallas kernels, forward(): pl.pallas_call(forward_kernel, grid_spec=pltpu.PrefetchScalarGridSpec(num...  26.2 us
    all_to_all x1, starting transfers between devices, everything(): lax.all_to_all(joined.reshape(nx * plane, PAIR // plane, width), ('x', 'z...  9.38 us
    all_to_all x1, starting transfers between devices, everything(): gathered = lax.all_to_all(rows, ('z', 'y'), 0, 0)  6.58 us
    pallas_call x1, Pallas kernels, join(): pl.pallas_call(join_kernel, in_specs=[hbm, hbm], out_specs=hbm, out_shape...  5.61 us
  transfers between devices with their start and end apart: 26, of which 12 were waited for; matrix products, arithmetic and copies ran while one was open for 1% of the time, Pallas kernels for 31%

profile of v1, /device:TPU:0, one launch (start us, length us, event | category | flops | bytes accessed | tf_op | source)
XLA Modules:
  0.0 173.6 jit_solution(1764468845459031983)
XLA Ops:
  0.6 0.7 pad_add_fusion.order.here
  1.3 13.1 %fwd.3 = bf16[4,256,2048]{2,1,0:T(8,128)(2,1)} custom-call(s32[2]{0:T(128)} %pad_add_fusion.order.here, bf16[1024,2048]{1,0:T(8,128)(2,1)} %bitcast.38, bf16[1024,2048]{1,0:T(8,128)(2,1)} %bitcast.41, bf16[1024,2048]{1,0:T(8,128)(2,1)} %bitcast.44, bf16[8,2,128,128]{3,2,1,0:T(8,128)(2,1)} %bitcast.47, f32[8,2,128]{2,1,0:T(2,128)} %bitcast.50, ...), custom_call_target="tpu_custom_call" | custom-call | flops 9126805504 | bytes 12582912 | tf_op jit(solution)/shard_map/fwd/pallas_call | solution.py:141
  14.4 0.1 collective-permute-start.9
  14.5 1.7 collective-permute-start.3
  16.2 1.6 collective-permute-start.1
  17.8 0.0 collective-permute-start
  17.8 23.7 %collective-permute-done.3.rest_9_ = bf16[256,2048]{1,0:T(8,128)(2,1)S(1)} collective-permute-done((bf16[256,2048]{1,0:T(8,128)(2,1)}, bf16[256,2048]{1,0:T(8,128)(2,1)S(1)}, u32[]{:S(2)}, u32[]{:S(2)}) %collective-permute-start.3) | collective-permute-done | bytes 1048608 | tf_op jit(solution)/shard_map/ppermute | solution.py:428
  41.6 0.5 collective-permute-start.4
  42.1 2.9 %collective-permute-start.6 = (bf16[128,2048]{1,0:T(8,128)(2,1)S(1)}, bf16[128,2048]{1,0:T(8,128)(2,1)}, u32[]{:S(2)}, u32[]{:S(2)}) collective-permute-start(bf16[128,2048]{1,0:T(8,128)(2,1)S(1)} %slice.33), channel_id=1, source_target_pairs={{0,6},{2,0},{4,2},{6,4},{1,7},{3,1},{5,3},{7,5},{8,14},{10,8},{12,... | collective-permute-start | bytes 1572872 | tf_op jit(solution)/shard_map/ppermute | solution.py:428
  45.0 0.5 collective-permute-start.8
  45.5 13.1 %fwd.2 = bf16[4,256,2048]{2,1,0:T(8,128)(2,1)} custom-call(s32[2]{0:T(128)} %pad_add_fusion.order.here, bf16[1024,2048]{1,0:T(8,128)(2,1)} %bitcast.39, bf16[1024,2048]{1,0:T(8,128)(2,1)} %bitcast.42, bf16[1024,2048]{1,0:T(8,128)(2,1)} %bitcast.45, bf16[8,2,128,128]{3,2,1,0:T(8,128)(2,1)} %bitcast.48, f32[8,2,128]{2,1,0:T(2,128)} %bitcast.51, ...), custom_call_target="tpu_custom_call" | custom-call | flops 9126805504 | bytes 12582912 | tf_op jit(solution)/shard_map/fwd/pallas_call | solution.py:141
  58.6 5.6 %join.1 = bf16[16,64,2048]{2,1,0:T(8,128)(2,1)} custom-call(bf16[16,64,2048]{2,1,0:T(8,128)(2,1)} %bitcast.33, bf16[16,64,2048]{2,1,0:T(8,128)(2,1)} %bitcast.12.b_hbm), custom_call_target="tpu_custom_call" | custom-call | flops 2097152 | bytes 12582912 | tf_op jit(solution)/shard_map/join/pallas_call | solution.py:349
  64.3 9.4 %all-to-all-start = ((bf16[64,16,2048]{2,1,0:T(8,128)(2,1)}), bf16[64,16,2048]{2,1,0:T(8,128)(2,1)}, u32[]{:S(2)}, u32[]{:S(2)}) async-start(bf16[64,16,2048]{2,1,0:T(8,128)(2,1)} %bitcast.32), calls=%async_computation | async-start | bytes 8388608 | tf_op jit(solution)/shard_map/all_to_all | solution.py:520
  73.7 0.1 collective-permute-start.5
  73.8 0.5 collective-permute-start.7
  74.3 1.6 collective-permute-done.5.rest_2_
  75.9 0.7 collective-permute-done.7.rest_3_
  76.6 0.1 copy-done.4
  76.7 0.7 copy-done.5
  77.4 28.6 %bwd.1 = (bf16[1024,2048]{1,0:T(8,128)(2,1)}, bf16[1024,2048]{1,0:T(8,128)(2,1)}, bf16[8,16,1152]{2,1,0:T(8,128)(2,1)}) custom-call(s32[2]{0:T(128)} %pad_add_fusion.order.here, bf16[1024,2048]{1,0:T(8,128)(2,1)} %bitcast.40, bf16[1024,2048]{1,0:T(8,128)(2,1)} %bitcast.43, bf16[1024,2048]{1,0:T(8,128)(2,1)} %bitcast.46, bf16[8,2,128,128]{3,2,1,0:T(8,128)(2,1)} %bitcast.49, ...), custom_call_target="tpu_custom_call" | custom-call | flops 20401094656 | bytes 29360128 | tf_op jit(solution)/shard_map/bwd/pallas_call | solution.py:383
  106.0 0.9 slice.27
  106.9 0.2 collective-permute-start.10
  107.1 1.2 collective-permute-done.10
  108.4 1.0 convert_add_fusion
  109.3 3.0 %collective-permute-start.13 = (bf16[16,1152]{1,0:T(8,128)(2,1)S(1)}, bf16[16,1152]{1,0:T(8,128)(2,1)S(1)}, u32[]{:S(2)}, u32[]{:S(2)}) collective-permute-start(bf16[16,1152]{1,0:T(8,128)(2,1)S(1)} %get-tuple-element.23), channel_id=1, source_target_pairs={{0,6},{2,0},{4,2},{6,4},{1,7},{3,1},{5,3},{7,5},{8,14},{10,8},{12,... | collective-permute-start | bytes 110600 | tf_op jit(solution)/shard_map/ppermute | solution.py:428
  112.3 2.2 %collective-permute-start.11 = (bf16[16,1152]{1,0:T(8,128)(2,1)S(1)}, bf16[16,1152]{1,0:T(8,128)(2,1)S(1)}, u32[]{:S(2)}, u32[]{:S(2)}) collective-permute-start(bf16[16,1152]{1,0:T(8,128)(2,1)S(1)} %get-tuple-element.21), channel_id=1, source_target_pairs={{0,4},{2,6},{4,0},{6,2},{1,5},{3,7},{5,1},{7,3},{8,12},{10,14},{12... | collective-permute-start | bytes 110600 | tf_op jit(solution)/shard_map/ppermute | solution.py:428
  114.5 10.5 %collective-permute-done.13 = bf16[16,1152]{1,0:T(8,128)(2,1)S(1)} collective-permute-done((bf16[16,1152]{1,0:T(8,128)(2,1)S(1)}, bf16[16,1152]{1,0:T(8,128)(2,1)S(1)}, u32[]{:S(2)}, u32[]{:S(2)}) %collective-permute-start.13) | collective-permute-done | bytes 36896 | tf_op jit(solution)/shard_map/ppermute | solution.py:428
  125.0 1.8 %collective-permute-done.12 = bf16[16,1152]{1,0:T(8,128)(2,1)S(1)} collective-permute-done((bf16[16,1152]{1,0:T(8,128)(2,1)S(1)}, bf16[16,1152]{1,0:T(8,128)(2,1)S(1)}, u32[]{:S(2)}, u32[]{:S(2)}) %collective-permute-start.12) | collective-permute-done | bytes 36896 | tf_op jit(solution)/shard_map/ppermute | solution.py:428
  126.9 1.9 %collective-permute-start.16 = (bf16[16,1152]{1,0:T(8,128)(2,1)S(1)}, bf16[16,1152]{1,0:T(8,128)(2,1)S(1)}, u32[]{:S(2)}, u32[]{:S(2)}) collective-permute-start(bf16[16,1152]{1,0:T(8,128)(2,1)S(1)} %fusion), channel_id=1, source_target_pairs={{0,24},{8,0},{16,8},{24,16},{1,25},{9,1},{17,9},{25,17},{2,26},{10... | collective-permute-start | bytes 110600 | tf_op jit(solution)/shard_map/ppermute | solution.py:428
  128.7 0.2 collective-permute-start.15
  129.0 2.9 %collective-permute-start.14 = (bf16[16,1152]{1,0:T(8,128)(2,1)S(1)}, bf16[16,1152]{1,0:T(8,128)(2,1)S(1)}, u32[]{:S(2)}, u32[]{:S(2)}) collective-permute-start(bf16[16,1152]{1,0:T(8,128)(2,1)S(1)} %fusion), channel_id=1, source_target_pairs={{0,16},{8,24},{16,0},{24,8},{1,17},{9,25},{17,1},{25,9},{2,18},{10... | collective-permute-start | bytes 110600 | tf_op jit(solution)/shard_map/ppermute | solution.py:428
  131.9 3.4 %row_sum.1 = bf16[16,16,2048]{2,1,0:T(8,128)(2,1)} custom-call(bf16[64,16,2048]{2,1,0:T(8,128)(2,1)} %all-to-all-done.x_hbm), custom_call_target="tpu_custom_call" | custom-call | flops 2097152 | bytes 6291456 | tf_op jit(solution)/shard_map/row_sum/pallas_call | solution.py:462
  135.3 6.6 %all-to-all-start.1 = ((bf16[16,16,2048]{2,1,0:T(8,128)(2,1)}), bf16[16,16,2048]{2,1,0:T(8,128)(2,1)S(1)}, u32[]{:S(2)}, u32[]{:S(2)}) async-start(bf16[16,16,2048]{2,1,0:T(8,128)(2,1)} %row_sum.1), calls=%async_computation.1 | async-start | bytes 2097152 | tf_op jit(solution)/shard_map/all_to_all | solution.py:544
  141.9 3.2 %collective-permute-start.19 = (bf16[16,1152]{1,0:T(8,128)(2,1)S(1)}, bf16[16,1152]{1,0:T(8,128)(2,1)S(1)}, u32[]{:S(2)}, u32[]{:S(2)}) collective-permute-start(bf16[16,1152]{1,0:T(8,128)(2,1)S(1)} %add_add_fusion.1), channel_id=1, source_target_pairs={{0,96},{32,0},{64,32},{96,64},{1,97},{33,1},{65,33},{97,65},{2,98}... | collective-permute-start | bytes 110600 | tf_op jit(solution)/shard_map/ppermute | solution.py:428
  145.1 2.3 %collective-permute-start.17 = (bf16[16,1152]{1,0:T(8,128)(2,1)S(1)}, bf16[16,1152]{1,0:T(8,128)(2,1)S(1)}, u32[]{:S(2)}, u32[]{:S(2)}) collective-permute-start(bf16[16,1152]{1,0:T(8,128)(2,1)S(1)} %add_add_fusion.1), channel_id=1, source_target_pairs={{0,64},{32,96},{64,0},{96,32},{1,65},{33,97},{65,1},{97,33},{2,66}... | collective-permute-start | bytes 110600 | tf_op jit(solution)/shard_map/ppermute | solution.py:428
  147.5 7.8 %collective-permute-done.19 = bf16[16,1152]{1,0:T(8,128)(2,1)S(1)} collective-permute-done((bf16[16,1152]{1,0:T(8,128)(2,1)S(1)}, bf16[16,1152]{1,0:T(8,128)(2,1)S(1)}, u32[]{:S(2)}, u32[]{:S(2)}) %collective-permute-start.19) | collective-permute-done | bytes 36896 | tf_op jit(solution)/shard_map/ppermute | solution.py:428
  155.2 1.0 collective-permute-done.18
  156.3 5.3 %collective-permute-start.22 = (bf16[16,1152]{1,0:T(8,128)(2,1)S(1)}, bf16[16,1152]{1,0:T(8,128)(2,1)S(1)}, u32[]{:S(2)}, u32[]{:S(2)}) collective-permute-start(bf16[16,1152]{1,0:T(8,128)(2,1)S(1)} %add_add_fusion), channel_id=1, source_target_pairs={{0,6},{2,0},{4,2},{6,4},{1,7},{3,1},{5,3},{7,5},{8,14},{10,8},{12,... | collective-permute-start | bytes 110600 | tf_op jit(solution)/shard_map/ppermute | solution.py:428
  161.5 0.4 collective-permute-start.21
  162.0 0.5 collective-permute-start.20
  162.5 0.7 collective-permute-done.22
  163.2 3.9 %collective-permute-done.21 = bf16[16,1152]{1,0:T(8,128)(2,1)S(1)} collective-permute-done((bf16[16,1152]{1,0:T(8,128)(2,1)S(1)}, bf16[16,1152]{1,0:T(8,128)(2,1)S(1)}, u32[]{:S(2)}, u32[]{:S(2)}) %collective-permute-start.21) | collective-permute-done | bytes 36896 | tf_op jit(solution)/shard_map/ppermute | solution.py:428
  167.0 0.4 collective-permute-done.20
  167.4 0.1 collective-permute-start.23
  167.5 1.4 collective-permute-done.23.theirs_ref
  168.9 0.7 copy-done.3
  169.5 2.4 %unpack.1 = (f32[16,128,128]{2,1,0:T(8,128)}, f32[16,128]{1,0:T(8,128)}, f32[16,128]{1,0:T(8,128)}, f32[16,128]{1,0:T(8,128)}) custom-call(s32[2]{0:T(128)} %pad_add_fusion.order.here, bf16[4,16,1152]{2,1,0:T(8,128)(2,1)} %copy-done, bf16[4,16,1152]{2,1,0:T(8,128)(2,1)} %copy-done.3), custom_call_target="tpu_custom_call" | custom-call | flops 1000000 | bytes 1000000 | tf_op jit(solution)/shard_map/unpack/pallas_call | solution.py:313
  172.0 1.6 bitcast_convert_fusion
  (33 shorter events, 0.3 us)
Async XLA Ops:
  14.4 30.6 %collective-permute-start.9 = (bf16[4,256,2048]{2,1,0:T(8,128)(2,1)}, bf16[4,256,2048]{2,1,0:T(8,128)(2,1)}, u32[]{:S(2)}, u32[]{:S(2)}) collective-permute-start(bf16[4,256,2048]{2,1,0:T(8,128)(2,1)} %fwd.3), channel_id=1, source_target_pairs={{0,1},{1,0},{2,3},{3,2},{4,5},{5,4},{6,7},{7,6},{8,9},{9,8},{10,11... | collective-permute-start | bytes 12582920 | tf_op jit(solution)/shard_map/ppermute | solution.py:428
  14.5 27.0 %collective-permute-start.3 = (bf16[256,2048]{1,0:T(8,128)(2,1)}, bf16[256,2048]{1,0:T(8,128)(2,1)S(1)}, u32[]{:S(2)}, u32[]{:S(2)}) collective-permute-start(bf16[256,2048]{1,0:T(8,128)(2,1)} %rest_5_.1), channel_id=1, source_target_pairs={{0,2},{2,4},{4,6},{6,0},{1,3},{3,5},{5,7},{7,1},{8,10},{10,12},{12... | collective-permute-start | bytes 3145736 | tf_op jit(solution)/shard_map/ppermute | solution.py:428
  16.2 25.8 %collective-permute-start.1 = (bf16[256,2048]{1,0:T(8,128)(2,1)}, bf16[256,2048]{1,0:T(8,128)(2,1)S(1)}, u32[]{:S(2)}, u32[]{:S(2)}) collective-permute-start(bf16[256,2048]{1,0:T(8,128)(2,1)} %rest_5_.1), channel_id=1, source_target_pairs={{0,6},{2,0},{4,2},{6,4},{1,7},{3,1},{5,3},{7,5},{8,14},{10,8},{12,... | collective-permute-start | bytes 3145736 | tf_op jit(solution)/shard_map/ppermute | solution.py:428
  17.8 56.4 %collective-permute-start = (bf16[256,2048]{1,0:T(8,128)(2,1)}, bf16[256,2048]{1,0:T(8,128)(2,1)}, u32[]{:S(2)}, u32[]{:S(2)}) collective-permute-start(bf16[256,2048]{1,0:T(8,128)(2,1)} %rest_5_.1), channel_id=1, source_target_pairs={{0,1},{1,0},{2,3},{3,2},{4,5},{5,4},{6,7},{7,6},{8,9},{9,8},{10,11... | collective-permute-start | bytes 3145736 | tf_op jit(solution)/shard_map/ppermute | solution.py:428
  41.5 17.1 %copy-start.1 = (bf16[256,2048]{1,0:T(8,128)(2,1)}, bf16[256,2048]{1,0:T(8,128)(2,1)S(1)}, u32[]{:S(2)}) copy-start(bf16[256,2048]{1,0:T(8,128)(2,1)S(1)} %collective-permute-done.3.rest_9_) | copy-start | bytes 3145732
  41.6 32.1 %collective-permute-start.4 = (bf16[128,2048]{1,0:T(8,128)(2,1)S(1)}, bf16[128,2048]{1,0:T(8,128)(2,1)}, u32[]{:S(2)}, u32[]{:S(2)}) collective-permute-start(bf16[128,2048]{1,0:T(8,128)(2,1)S(1)} %slice.32), channel_id=1, source_target_pairs={{0,2},{2,4},{4,6},{6,0},{1,3},{3,5},{5,7},{7,1},{8,10},{10,12},{12... | collective-permute-start | bytes 1572872 | tf_op jit(solution)/shard_map/ppermute | solution.py:428
  42.0 16.6 %copy-start.2 = (bf16[256,2048]{1,0:T(8,128)(2,1)}, bf16[256,2048]{1,0:T(8,128)(2,1)S(1)}, u32[]{:S(2)}) copy-start(bf16[256,2048]{1,0:T(8,128)(2,1)S(1)} %collective-permute-done.1.rest_6_) | copy-start | bytes 3145732
  42.1 31.7 %collective-permute-start.6 = (bf16[128,2048]{1,0:T(8,128)(2,1)S(1)}, bf16[128,2048]{1,0:T(8,128)(2,1)}, u32[]{:S(2)}, u32[]{:S(2)}) collective-permute-start(bf16[128,2048]{1,0:T(8,128)(2,1)S(1)} %slice.33), channel_id=1, source_target_pairs={{0,6},{2,0},{4,2},{6,4},{1,7},{3,1},{5,3},{7,5},{8,14},{10,8},{12,... | collective-permute-start | bytes 1572872 | tf_op jit(solution)/shard_map/ppermute | solution.py:428
  45.0 29.3 %collective-permute-start.2 = (bf16[256,2048]{1,0:T(8,128)(2,1)S(1)}, bf16[256,2048]{1,0:T(8,128)(2,1)}, u32[]{:S(2)}, u32[]{:S(2)}) collective-permute-start(bf16[256,2048]{1,0:T(8,128)(2,1)S(1)} %collective-permute-done.1.rest_6_), channel_id=1, source_target_pairs={{0,1},{1,0},{2,3},{3,2},{4,5},{5,4},{6,7},{7,6},{8,9},{9,8},{10,11... | collective-permute-start | bytes 3145736 | tf_op jit(solution)/shard_map/ppermute | solution.py:428
  45.0 31.6 %collective-permute-start.8 = (bf16[256,2048]{1,0:T(8,128)(2,1)S(1)}, bf16[256,2048]{1,0:T(8,128)(2,1)}, u32[]{:S(2)}, u32[]{:S(2)}) collective-permute-start(bf16[256,2048]{1,0:T(8,128)(2,1)S(1)} %collective-permute-done.3.rest_9_), channel_id=1, source_target_pairs={{0,1},{1,0},{2,3},{3,2},{4,5},{5,4},{6,7},{7,6},{8,9},{9,8},{10,11... | collective-permute-start | bytes 3145736 | tf_op jit(solution)/shard_map/ppermute | solution.py:428
  64.3 67.6 %all-to-all-start = ((bf16[64,16,2048]{2,1,0:T(8,128)(2,1)}), bf16[64,16,2048]{2,1,0:T(8,128)(2,1)}, u32[]{:S(2)}, u32[]{:S(2)}) async-start(bf16[64,16,2048]{2,1,0:T(8,128)(2,1)} %bitcast.32), calls=%async_computation | async-start | bytes 8388608 | tf_op jit(solution)/shard_map/all_to_all | solution.py:520
  73.7 2.2 %collective-permute-start.5 = (bf16[128,2048]{1,0:T(8,128)(2,1)}, bf16[128,2048]{1,0:T(8,128)(2,1)S(1)}, u32[]{:S(2)}, u32[]{:S(2)}) collective-permute-start(bf16[128,2048]{1,0:T(8,128)(2,1)} %collective-permute-done.4.rest_7_), channel_id=1, source_target_pairs={{0,1},{1,0},{2,3},{3,2},{4,5},{5,4},{6,7},{7,6},{8,9},{9,8},{10,11... | collective-permute-start | bytes 1572872 | tf_op jit(solution)/shard_map/ppermute | solution.py:428
  73.8 2.8 %collective-permute-start.7 = (bf16[128,2048]{1,0:T(8,128)(2,1)}, bf16[128,2048]{1,0:T(8,128)(2,1)S(1)}, u32[]{:S(2)}, u32[]{:S(2)}) collective-permute-start(bf16[128,2048]{1,0:T(8,128)(2,1)} %collective-permute-done.6.rest_8_), channel_id=1, source_target_pairs={{0,1},{1,0},{2,3},{3,2},{4,5},{5,4},{6,7},{7,6},{8,9},{9,8},{10,11... | collective-permute-start | bytes 1572872 | tf_op jit(solution)/shard_map/ppermute | solution.py:428
  75.9 0.8 copy-start.4
  76.6 0.8 copy-start.5
  106.9 1.5 collective-permute-start.10
  109.3 15.7 %collective-permute-start.13 = (bf16[16,1152]{1,0:T(8,128)(2,1)S(1)}, bf16[16,1152]{1,0:T(8,128)(2,1)S(1)}, u32[]{:S(2)}, u32[]{:S(2)}) collective-permute-start(bf16[16,1152]{1,0:T(8,128)(2,1)S(1)} %get-tuple-element.23), channel_id=1, source_target_pairs={{0,6},{2,0},{4,2},{6,4},{1,7},{3,1},{5,3},{7,5},{8,14},{10,8},{12,... | collective-permute-start | bytes 110600 | tf_op jit(solution)/shard_map/ppermute | solution.py:428
  112.3 14.5 %collective-permute-start.12 = (bf16[16,1152]{1,0:T(8,128)(2,1)S(1)}, bf16[16,1152]{1,0:T(8,128)(2,1)S(1)}, u32[]{:S(2)}, u32[]{:S(2)}) collective-permute-start(bf16[16,1152]{1,0:T(8,128)(2,1)S(1)} %get-tuple-element.22), channel_id=1, source_target_pairs={{0,2},{2,4},{4,6},{6,0},{1,3},{3,5},{5,7},{7,1},{8,10},{10,12},{12... | collective-permute-start | bytes 110600 | tf_op jit(solution)/shard_map/ppermute | solution.py:428
  112.3 14.5 %collective-permute-start.11 = (bf16[16,1152]{1,0:T(8,128)(2,1)S(1)}, bf16[16,1152]{1,0:T(8,128)(2,1)S(1)}, u32[]{:S(2)}, u32[]{:S(2)}) collective-permute-start(bf16[16,1152]{1,0:T(8,128)(2,1)S(1)} %get-tuple-element.21), channel_id=1, source_target_pairs={{0,4},{2,6},{4,0},{6,2},{1,5},{3,7},{5,1},{7,3},{8,12},{10,14},{12... | collective-permute-start | bytes 110600 | tf_op jit(solution)/shard_map/ppermute | solution.py:428
  126.9 15.0 %collective-permute-start.16 = (bf16[16,1152]{1,0:T(8,128)(2,1)S(1)}, bf16[16,1152]{1,0:T(8,128)(2,1)S(1)}, u32[]{:S(2)}, u32[]{:S(2)}) collective-permute-start(bf16[16,1152]{1,0:T(8,128)(2,1)S(1)} %fusion), channel_id=1, source_target_pairs={{0,24},{8,0},{16,8},{24,16},{1,25},{9,1},{17,9},{25,17},{2,26},{10... | collective-permute-start | bytes 110600 | tf_op jit(solution)/shard_map/ppermute | solution.py:428
  128.7 13.1 %collective-permute-start.15 = (bf16[16,1152]{1,0:T(8,128)(2,1)S(1)}, bf16[16,1152]{1,0:T(8,128)(2,1)S(1)}, u32[]{:S(2)}, u32[]{:S(2)}) collective-permute-start(bf16[16,1152]{1,0:T(8,128)(2,1)S(1)} %fusion), channel_id=1, source_target_pairs={{0,8},{8,16},{16,24},{24,0},{1,9},{9,17},{17,25},{25,1},{2,10},{10... | collective-permute-start | bytes 110600 | tf_op jit(solution)/shard_map/ppermute | solution.py:428
  129.0 12.9 %collective-permute-start.14 = (bf16[16,1152]{1,0:T(8,128)(2,1)S(1)}, bf16[16,1152]{1,0:T(8,128)(2,1)S(1)}, u32[]{:S(2)}, u32[]{:S(2)}) collective-permute-start(bf16[16,1152]{1,0:T(8,128)(2,1)S(1)} %fusion), channel_id=1, source_target_pairs={{0,16},{8,24},{16,0},{24,8},{1,17},{9,25},{17,1},{25,9},{2,18},{10... | collective-permute-start | bytes 110600 | tf_op jit(solution)/shard_map/ppermute | solution.py:428
  135.3 36.7 %all-to-all-start.1 = ((bf16[16,16,2048]{2,1,0:T(8,128)(2,1)}), bf16[16,16,2048]{2,1,0:T(8,128)(2,1)S(1)}, u32[]{:S(2)}, u32[]{:S(2)}) async-start(bf16[16,16,2048]{2,1,0:T(8,128)(2,1)} %row_sum.1), calls=%async_computation.1 | async-start | bytes 2097152 | tf_op jit(solution)/shard_map/all_to_all | solution.py:544
  141.9 13.3 %collective-permute-start.19 = (bf16[16,1152]{1,0:T(8,128)(2,1)S(1)}, bf16[16,1152]{1,0:T(8,128)(2,1)S(1)}, u32[]{:S(2)}, u32[]{:S(2)}) collective-permute-start(bf16[16,1152]{1,0:T(8,128)(2,1)S(1)} %add_add_fusion.1), channel_id=1, source_target_pairs={{0,96},{32,0},{64,32},{96,64},{1,97},{33,1},{65,33},{97,65},{2,98}... | collective-permute-start | bytes 110600 | tf_op jit(solution)/shard_map/ppermute | solution.py:428
  145.1 11.1 %collective-permute-start.18 = (bf16[16,1152]{1,0:T(8,128)(2,1)S(1)}, bf16[16,1152]{1,0:T(8,128)(2,1)S(1)}, u32[]{:S(2)}, u32[]{:S(2)}) collective-permute-start(bf16[16,1152]{1,0:T(8,128)(2,1)S(1)} %add_add_fusion.1), channel_id=1, source_target_pairs={{0,32},{32,64},{64,96},{96,0},{1,33},{33,65},{65,97},{97,1},{2,34}... | collective-permute-start | bytes 110600 | tf_op jit(solution)/shard_map/ppermute | solution.py:428
  145.1 11.1 %collective-permute-start.17 = (bf16[16,1152]{1,0:T(8,128)(2,1)S(1)}, bf16[16,1152]{1,0:T(8,128)(2,1)S(1)}, u32[]{:S(2)}, u32[]{:S(2)}) collective-permute-start(bf16[16,1152]{1,0:T(8,128)(2,1)S(1)} %add_add_fusion.1), channel_id=1, source_target_pairs={{0,64},{32,96},{64,0},{96,32},{1,65},{33,97},{65,1},{97,33},{2,66}... | collective-permute-start | bytes 110600 | tf_op jit(solution)/shard_map/ppermute | solution.py:428
  156.3 6.9 %collective-permute-start.22 = (bf16[16,1152]{1,0:T(8,128)(2,1)S(1)}, bf16[16,1152]{1,0:T(8,128)(2,1)S(1)}, u32[]{:S(2)}, u32[]{:S(2)}) collective-permute-start(bf16[16,1152]{1,0:T(8,128)(2,1)S(1)} %add_add_fusion), channel_id=1, source_target_pairs={{0,6},{2,0},{4,2},{6,4},{1,7},{3,1},{5,3},{7,5},{8,14},{10,8},{12,... | collective-permute-start | bytes 110600 | tf_op jit(solution)/shard_map/ppermute | solution.py:428
  161.5 5.5 %collective-permute-start.21 = (bf16[16,1152]{1,0:T(8,128)(2,1)S(1)}, bf16[16,1152]{1,0:T(8,128)(2,1)S(1)}, u32[]{:S(2)}, u32[]{:S(2)}) collective-permute-start(bf16[16,1152]{1,0:T(8,128)(2,1)S(1)} %add_add_fusion), channel_id=1, source_target_pairs={{0,4},{2,6},{4,0},{6,2},{1,5},{3,7},{5,1},{7,3},{8,12},{10,14},{12... | collective-permute-start | bytes 110600 | tf_op jit(solution)/shard_map/ppermute | solution.py:428
  162.0 5.4 %collective-permute-start.20 = (bf16[16,1152]{1,0:T(8,128)(2,1)S(1)}, bf16[16,1152]{1,0:T(8,128)(2,1)S(1)}, u32[]{:S(2)}, u32[]{:S(2)}) collective-permute-start(bf16[16,1152]{1,0:T(8,128)(2,1)S(1)} %add_add_fusion), channel_id=1, source_target_pairs={{0,2},{2,4},{4,6},{6,0},{1,3},{3,5},{5,7},{7,1},{8,10},{10,12},{12... | collective-permute-start | bytes 110600 | tf_op jit(solution)/shard_map/ppermute | solution.py:428
  167.4 1.5 copy-start
  167.4 1.5 collective-permute-start.23
  168.9 0.7 copy-start.3
